TPU v7x, 512 devices: a whole 4x8x8 slice. The times are simulated.
512 devices in a mesh: sp: 32 (over z, x), dp: 16 (over y, core).
Axes of the slice: x: 4, y: 8, z: 8, core: 2. Of those that a mesh axis runs over, the one named last changes fastest.
Arguments:
- queries: bfloat16 [16, 4096, 2048], P('dp', 'sp'), may hold values from -6 to 6
- keys: bfloat16 [16, 4096, 2048], P('dp', 'sp'), may hold values from -6 to 6
- values: bfloat16 [16, 4096, 2048], P('dp', 'sp'), may hold values from -6 to 6
- gate_totals: float32 [16, 4096, 32], P('dp', 'sp'), may hold values from -4096 to 0, as said below
- w_out: bfloat16 [2048, 2048], P(None, 'dp'), may hold values from -1 to 1
Outputs:
- mixed: bfloat16 [16, 4096, 2048], P('dp', 'sp')
Inputs may be any that keep to these rules, and one draw needn't show every extreme that they name: `gate_totals`: never rising along a sequence.
All inputs are finite; a program needn't handle non-finite values.
Results may differ from a plain program's by a relative error of at most 0.0053.
Values may be sent and summed in bfloat16 or wider, within the bound.
No kernel may reach another device: no remote copies, remote signals or barrier semaphores. Data moves between devices by JAX's collectives and lax.ppermute only.
A program may use at most 64 MiB of HBM per device.

v0:
```python
import jax
import jax.numpy as jnp
from jax import lax
from jax.sharding import Mesh
from jax.sharding import PartitionSpec as P

HEAD_DIM = 64
SP = ("sp_0", "sp_1")


def in_one_piece(arrays, axis, split_dim, concat_dim, along):
    ends, at = ([], 0)
    for a in arrays[:-1]:
        at += a.shape[along]
        ends.append(at)
    both = jnp.concatenate(arrays, axis=along)
    return tuple(
        jnp.split(
            lax.all_to_all(both, axis, split_axis=split_dim, concat_axis=concat_dim, tiled=True),
            ends,
            axis=along,
        )
    )


def in_blocks(array, dim, length):
    before, after = (array.shape[:dim], array.shape[dim + 1 :])
    return jnp.moveaxis(array.reshape(*before, length, -1, *after), dim, 0)


def laid_out(parts, dim):
    dims = list(parts.shape[1:])
    dims[dim] *= parts.shape[0]
    return jnp.moveaxis(parts, 0, dim).reshape(dims)


def exchange_in_order(parts, axes, sequence):
    dims = [lax.axis_size(a) for a in axes]
    parts = parts.reshape(*dims, *parts.shape[1:])
    for k in sequence:
        parts = lax.all_to_all(parts, axes[k], split_axis=k, concat_axis=k, tiled=True)
    return parts.reshape(-1, *parts.shape[len(axes) :])


def one_axis_at_a_time(array, axes, sequence, split_dim, concat_dim):
    parts = in_blocks(array, split_dim, lax.axis_size(axes))
    return laid_out(exchange_in_order(parts, axes, sequence), concat_dim)


def attend(queries, key_rows, value_rows, totals):
    length = queries.shape[0]
    block_rows = min(length, 512)
    pieces = []
    for begin_row in range(0, length, block_rows):
        end_row = begin_row + block_rows
        scaled = queries[begin_row:end_row] * jnp.bfloat16(HEAD_DIM ** (-0.5))
        scores = jnp.einsum(
            "qhd,khd->hqk", scaled, key_rows[:end_row], preferred_element_type=jnp.float32
        )
        causal = jnp.arange(end_row)[None, :] <= (begin_row + jnp.arange(block_rows))[:, None]
        scores = jnp.where(
            causal[None],
            scores
            + jnp.transpose(totals[begin_row:end_row])[:, :, None]
            - jnp.transpose(totals[:end_row])[:, None, :],
            -jnp.inf,
        )
        biggest = jnp.max(scores, axis=-1, keepdims=True)
        expo = jnp.exp(scores - biggest)
        summed = jnp.sum(expo, axis=-1)
        weights = expo.astype(jnp.bfloat16)
        output = jnp.einsum(
            "hqk,khd->qhd", weights, value_rows[:end_row], preferred_element_type=jnp.float32
        )
        output = output / jnp.transpose(summed)[:, :, None]
        pieces.append(output.astype(jnp.bfloat16))
    return jnp.concatenate(pieces, axis=0).reshape(length, -1)


def local(queries, keys, values, gate_totals, w_out):
    moved = in_one_piece((queries, keys, values), SP, 2, 1, 0)
    totals = lax.all_to_all(gate_totals, SP, split_axis=2, concat_axis=1, tiled=True)
    held, length = (moved[0].shape[0], moved[0].shape[1])
    query_heads, key_heads, value_heads = [
        part_array[0].reshape(length, -1, HEAD_DIM) for part_array in moved
    ]
    outputs = [attend(query_heads, key_heads, value_heads, totals[0])]
    attended = jnp.stack(outputs, axis=0)
    local_rows = one_axis_at_a_time(attended, SP, (0, 1), 1, 2)
    flat_rows = local_rows.reshape(-1, local_rows.shape[2])
    mixed = jnp.dot(
        flat_rows,
        lax.all_gather(w_out, "dp", axis=1, tiled=True),
        preferred_element_type=jnp.float32,
    )
    return mixed.astype(jnp.bfloat16).reshape(local_rows.shape[0], local_rows.shape[1], -1)


def solution(mesh):
    torus = Mesh(mesh.devices.reshape(8, 4, mesh.shape["dp"]), ("sp_0", "sp_1", "dp"))
    in_specs = (
        P("dp", SP, None),
        P("dp", SP, None),
        P("dp", SP, None),
        P("dp", SP, None),
        P(None, "dp"),
    )
    out_specs = P("dp", SP, None)
    return jax.shard_map(local, mesh=torus, in_specs=in_specs, out_specs=out_specs, check_vma=False)
```

profile of v0, /device:TPU:40, one launch (start us, length us, event | category | flops | bytes accessed | tf_op | source)
XLA Modules:
  0.0 165.8 jit_solution(11450211119789612422)
XLA Ops:
  6.5 0.7 all-gather.2.cloned.1.call-update
  7.3 13.2 %all-to-all-start.1 = ((f32[1,128,32]{1,0,2:T(1,128)}), f32[1,128,32]{1,0,2:T(1,128)S(1)}, u32[]{:S(2)}, u32[]{:S(2)}) async-start(f32[1,128,32]{1,0,2:T(1,128)} %bitcast.401), calls=%async_computation.1 | async-start | bytes 32768 | tf_op jit(solution)/shard_map/all_to_all | solution.py:82
  20.4 2.4 %copy.34 = bf16[1,128,2048]{1,0,2:T(2,128)(2,1)S(1)} copy(bf16[1,128,2048]{2,1,0:T(8,128)(2,1)} %param.5) | data formatting | bytes 1048576 | tf_op args[0]
  22.8 2.4 %copy.35 = bf16[1,128,2048]{1,0,2:T(2,128)(2,1)S(1)} copy(bf16[1,128,2048]{2,1,0:T(8,128)(2,1)} %param.6) | data formatting | bytes 1048576 | tf_op args[1]
  25.2 2.4 %copy.36 = bf16[1,128,2048]{1,0,2:T(2,128)(2,1)S(1)} copy(bf16[1,128,2048]{2,1,0:T(8,128)(2,1)} %param.7) | data formatting | bytes 1048576 | tf_op args[2]
  27.5 4.5 %pad_maximum_fusion = bf16[3,128,2048]{1,0,2:T(4,128)(2,1)} fusion(bf16[1,128,2048]{1,0,2:T(2,128)(2,1)S(1)} %copy.36, bf16[1,128,2048]{1,0,2:T(2,128)(2,1)S(1)} %copy.35, bf16[1,128,2048]{1,0,2:T(2,128)(2,1)S(1)} %copy.34), kind=kLoop, calls=%fused_computation.43 | loop fusion | flops 4718592 | bytes 3145728 | tf_op jit(solution)/shard_map/concatenate | solution.py:16
  32.1 10.0 %all-to-all-start = ((bf16[3,128,2048]{1,0,2:T(4,128)(2,1)}), bf16[3,128,2048]{1,0,2:T(4,128)(2,1)S(1)}, u32[]{:S(2)}, u32[]{:S(2)}) async-start(bf16[3,128,2048]{1,0,2:T(4,128)(2,1)} %pad_maximum_fusion), calls=%async_computation | async-start | bytes 4194304 | tf_op jit(solution)/shard_map/all_to_all | solution.py:19
  42.2 49.3 %all-to-all-done = bf16[3,128,2048]{1,0,2:T(4,128)(2,1)S(1)} async-done(((bf16[3,128,2048]{1,0,2:T(4,128)(2,1)}), bf16[3,128,2048]{1,0,2:T(4,128)(2,1)S(1)}, u32[]{:S(2)}, u32[]{:S(2)}) %all-to-all-start) | async-done | bytes 1572896 | tf_op jit(solution)/shard_map/all_to_all | solution.py:19
  91.4 0.2 copy.37
  92.7 0.2 copy.50
  93.2 0.2 copy.53
  93.4 0.2 copy.51
  93.8 0.3 copy.56
  94.0 0.3 copy.54
  94.4 0.3 copy.59
  94.7 0.3 copy.57
  95.2 0.3 copy.62
  95.5 0.3 copy.60
  95.9 0.4 fusion.196
  96.3 0.2 fusion.137
  96.5 0.7 fusion.197
  97.2 0.5 fusion.30
  97.6 0.9 fusion.198
  98.5 0.6 fusion.21
  99.1 0.3 fusion.134
  99.4 0.5 fusion.130
  99.9 1.2 fusion.199
  101.1 0.7 fusion.11
  101.8 0.7 fusion.124
  102.5 0.9 fusion.100
  103.3 1.6 fusion.200
  105.0 0.8 fusion.6
  105.8 1.0 fusion.94
  106.8 1.7 %fusion.201 = (f32[512]{0:T(512)S(1)}, f32[512,3072]{1,0:T(8,128)S(1)}) fusion(f32[3072]{0:T(1024)S(1)} %slice_bitcast_fusion.1, f32[512]{0:T(512)S(1)} %get-tuple-element.31, bf16[8,8,24,128]{3,2,1,0:T(8,128)(2,1)S(1)} %bitcast.386, bf16[8,8,4,128]{3,2,1,0:T(4,128)(2,1)S(1)} %bitcast.394, s32[512]{0:T(512)S(1)} %iota_add_fusion.2), kind=kOutput, calls=%fused_computation.190 | convolution fusion | flops 209190400 | bytes 6768640 | tf_op jit(solution)/shard_map/qhd,khd->hqk/dot_general | solution.py:57
  108.5 1.0 fusion.4
  109.5 1.2 fusion.106
  110.7 2.0 %fusion.202 = (f32[512]{0:T(512)S(1)}, f32[512,3584]{1,0:T(8,128)S(1)}) fusion(f32[3584]{0:T(1024)S(1)} %slice_bitcast_fusion, f32[512]{0:T(512)S(1)} %get-tuple-element.30, bf16[8,8,28,128]{3,2,1,0:T(8,128)(2,1)S(1)} %bitcast.385, bf16[8,8,4,128]{3,2,1,0:T(4,128)(2,1)S(1)} %bitcast.393, s32[512]{0:T(512)S(1)} %iota_add_fusion.1), kind=kOutput, calls=%fused_computation.191 | convolution fusion | flops 244055552 | bytes 7884800 | tf_op jit(solution)/shard_map/qhd,khd->hqk/dot_general | solution.py:57
  112.7 1.1 fusion.2
  113.8 1.4 fusion.118
  115.2 2.2 %fusion.203 = (f32[512]{0:T(512)S(1)}, f32[512,4096]{1,0:T(8,128)S(1)}) fusion(f32[4096]{0:T(1024)S(1)} %bitcast.382, f32[512]{0:T(512)S(1)} %get-tuple-element.29, bf16[8,8,32,128]{3,2,1,0:T(8,128)(2,1)S(1)} %bitcast.384, bf16[8,8,4,128]{3,2,1,0:T(4,128)(2,1)S(1)} %bitcast.392, s32[512]{0:T(512)S(1)} %iota_add_fusion), kind=kOutput, calls=%fused_computation.192 | convolution fusion | flops 278920704 | bytes 9000960 | tf_op jit(solution)/shard_map/qhd,khd->hqk/dot_general | solution.py:57
  117.5 1.5 fusion
  119.0 1.6 fusion.112
  120.6 0.4 reshape_transpose_reshape_stack_reshape.3
  121.0 0.2 copy.63
  121.1 19.0 %all_to_all.40 = bf16[8,4,1,128,64]{3,1,4,2,0:T(4,128)(2,1)S(1)} all-to-all(bf16[8,4,1,128,64]{3,1,4,2,0:T(4,128)(2,1)S(1)} %copy.63), channel_id=1, replica_groups=mesh['sp_0'=8,'sp_1'=4,'dp'=16] {'sp_0'}, dimensions={0} | all-to-all | bytes 1048576 | tf_op jit(solution)/shard_map/all_to_all | solution.py:41
  140.2 0.3 copy.64
  140.5 12.8 %all_to_all.41 = bf16[8,4,1,128,64]{3,0,4,2,1:T(8,128)(2,1)S(1)} all-to-all(bf16[8,4,1,128,64]{3,0,4,2,1:T(8,128)(2,1)S(1)} %copy.64), channel_id=1, replica_groups=mesh['sp_0'=8,'sp_1'=4,'dp'=16] {'sp_1'}, dimensions={1} | all-to-all | bytes 1048576 | tf_op jit(solution)/shard_map/all_to_all | solution.py:41
  153.5 5.5 %fusion.26 = bf16[1,128,2048]{2,1,0:T(8,128)(2,1)} fusion(bf16[128,2048]{0,1:T(8,128)(2,1)S(1)} %bitcast.368, bf16[2048,2048]{1,0:T(8,128)(2,1)} %all-gather.2.cloned.1.call-done), kind=kOutput, calls=%fused_computation.41 | convolution fusion | flops 1074003968 | bytes 9437184 | tf_op jit(solution)/shard_map/dot_general | solution.py:91
  (41 shorter events, 1.7 us)
Async XLA Ops:
  6.5 146.9 %all-gather.2.cloned.1.call-start = ((), (), s32[]{:S(2)}) async-start(), calls=%async_computation.4 | async-start | bytes 8912896 | tf_op jit(solution)/shard_map/all_gather | solution.py:93
  7.3 24.8 %all-to-all-start.1 = ((f32[1,128,32]{1,0,2:T(1,128)}), f32[1,128,32]{1,0,2:T(1,128)S(1)}, u32[]{:S(2)}, u32[]{:S(2)}) async-start(f32[1,128,32]{1,0,2:T(1,128)} %bitcast.401), calls=%async_computation.1 | async-start | bytes 32768 | tf_op jit(solution)/shard_map/all_to_all | solution.py:82
  32.1 59.4 %all-to-all-start = ((bf16[3,128,2048]{1,0,2:T(4,128)(2,1)}), bf16[3,128,2048]{1,0,2:T(4,128)(2,1)S(1)}, u32[]{:S(2)}, u32[]{:S(2)}) async-start(bf16[3,128,2048]{1,0,2:T(4,128)(2,1)} %pad_maximum_fusion), calls=%async_computation | async-start | bytes 4194304 | tf_op jit(solution)/shard_map/all_to_all | solution.py:19
Sparse Core Ops, SparseCore 0:
  9.4 68.7 all-gather.1
where the time goes:
time: 166 us
  waiting for transfers between devices  50 us (30%)
  blocking collectives  31.8 us (19%)
  matrix products  23.7 us (14%)
  starting transfers between devices  23.1 us (14%)
  between operations  13.8 us (8%)
  local copies, waits for them, and re-layouts  12.3 us (7%)
  other arithmetic  11.1 us (7%)
    all_to_all x1, waiting for transfers between devices, in_one_piece(): lax.all_to_all(both, axis, split_axis=split_dim, concat_axis=concat_dim,...  49.3 us
    all_to_all x2, blocking collectives, exchange_in_order(): lax.all_to_all(parts, axes[k], split_axis=k, concat_axis=k, tiled=True)  31.8 us
    all_to_all x1, starting transfers between devices, local(): lax.all_to_all(gate_totals, SP, split_axis=2, concat_axis=1, tiled=True)  13.2 us
    dot_general x8, matrix products, attend(): jnp.einsum('qhd,khd->hqk', scaled, key_rows[:end_row], preferred_element_...  10.6 us
    all_to_all x1, starting transfers between devices, in_one_piece(): lax.all_to_all(both, axis, split_axis=split_dim, concat_axis=concat_dim,...  9.96 us
    dot_general x8, matrix products, attend(): jnp.einsum('hqk,khd->qhd', weights, value_rows[:end_row], preferred_eleme...  7.55 us
    unnamed x3, local copies, waits for them, and re-layouts  7.06 us
    reduce_sum x8, other arithmetic, attend(): summed = jnp.sum(expo, axis=-1)  6.48 us
  transfers between devices with their start and end apart: 3, of which 1 were waited for; matrix products, arithmetic and copies ran while one was open for 25% of the time, Pallas kernels for 0%

commit v1 on v0

v1 whole, which is shorter than its diff:
```python
import functools
import math

import jax
import jax.numpy as jnp
from jax import lax
from jax.experimental import pallas as pl
from jax.experimental.pallas import tpu as pltpu
from jax.sharding import Mesh
from jax.sharding import PartitionSpec as P

HD = 64
SP = ("sp_0", "sp_1")
LOG2E = math.log2(math.e)
F32 = jnp.float32
BF16 = jnp.bfloat16
TILE = 128
ROWS = 208
BLK = 512


def split3(x):
    a = x.astype(BF16)
    r = x - a.astype(F32)
    b = r.astype(BF16)
    c = (r - b.astype(F32)).astype(BF16)
    return a, b, c


def gate_rows(a, b, c):
    row = lax.broadcasted_iota(jnp.int32, (16, a.shape[1]), 0)
    a, b, c = (t.astype(F32) for t in (a, b, c))
    t = jnp.where(row == 0, a, jnp.where(row == 1, b, jnp.where(row == 2, c, 0.0)))
    return t.astype(BF16)


def pack_kernel(q_ref, k_ref, v_ref, g_ref, o_ref):
    heads = o_ref.shape[0]
    a, b, c = split3(jnp.transpose(g_ref[0]))
    a, b, c = (t.astype(F32) for t in (a, b, c))
    for p in range(heads // 2):
        cols = slice(2 * p * HD, 2 * (p + 1) * HD)
        for ref, at in ((k_ref, 0), (q_ref, 80), (v_ref, 144)):
            t = jnp.transpose(ref[0, :, cols])
            o_ref[2 * p, at : at + HD, :] = t[:HD]
            o_ref[2 * p + 1, at : at + HD, :] = t[HD:]
    for h in range(heads):
        o_ref[h, 64:80, :] = gate_rows(a[h : h + 1], b[h : h + 1], c[h : h + 1])


def pack(q, k, v, g):
    heads = q.shape[2] // HD
    vm = pl.BlockSpec(memory_space=pltpu.VMEM)
    return pl.pallas_call(
        pack_kernel,
        out_shape=jax.ShapeDtypeStruct((heads, ROWS, q.shape[1]), BF16),
        in_specs=[vm] * 4,
        out_specs=vm,
        cost_estimate=pl.CostEstimate(flops=10**7, bytes_accessed=4 * 10**6, transcendentals=0),
        name="pack",
    )(q, k, v, g)


def attend_kernel(r_ref, o_ref, kaug, qaug, vaug, s0, s1, acc, cref):
    nb = kaug.shape[0]
    per = BLK // TILE

    rows64 = lax.broadcasted_iota(jnp.int32, (64, BLK), 0)
    ones_rows = jnp.where(rows64 < 3, 1.0, 0.0).astype(BF16)
    vrow = lax.broadcasted_iota(jnp.int32, (16, BLK), 0)
    vones = jnp.where(vrow < 1, 1.0, 0.0).astype(BF16)

    def prepare(c, _):
        gs = []
        for t in range(per):
            g = r_ref[c * per + t, 64:80, :].astype(F32)
            gs.append(g[0:1] + g[1:2] + g[2:3])
        ref = jnp.broadcast_to(gs[-1][:, TILE - 1 : TILE], (1, TILE))
        cref[c] = jnp.broadcast_to(jnp.concatenate([ref * LOG2E] * per, axis=1), (8, BLK))
        for t in range(per):
            j = c * per + t
            lanes = slice(t * TILE, (t + 1) * TILE)
            kt = r_ref[j, 0:64, :]
            bias = gate_rows(*split3((ref - gs[t]) * LOG2E))
            lo = jnp.concatenate([kt, kt], axis=0)
            hi = jnp.concatenate([kt, bias, jnp.zeros((48, TILE), BF16)], axis=0)
            kaug[c, lanes, 0:128] = jnp.transpose(lo)
            kaug[c, lanes, 128:256] = jnp.transpose(hi)
            q1, q2, q3 = split3(r_ref[j, 80:144, :].astype(F32) * (LOG2E * HD**-0.5))
            qaug[c, 0:64, lanes] = q1
            qaug[c, 64:128, lanes] = q2
            qaug[c, 128:192, lanes] = q3
            vaug[c, 0:64, lanes] = r_ref[j, 144:208, :]
        qaug[c, 192:256, :] = ones_rows
        vaug[c, 64:80, :] = vones
        return 0

    lax.fori_loop(0, nb, prepare, 0)

    def fold(s):
        return jnp.max(s.reshape(BLK // 8, 8, BLK), axis=0)

    def scores(i, c):
        return jnp.dot(kaug[c], qaug[i], preferred_element_type=F32)

    def diagonal(i, dst):
        s = scores(i, i)
        key = lax.broadcasted_iota(jnp.int32, (BLK, BLK), 0)
        query = lax.broadcasted_iota(jnp.int32, (BLK, BLK), 1)
        s = jnp.where(key <= query, s, -jnp.inf)
        dst[i] = s
        return fold(s)

    def weigh(c, m, src, i):
        mm = m - (cref[i] - cref[c])
        p = jnp.exp2(src[c].reshape(BLK // 8, 8, BLK) - mm[None])
        p = p.reshape(BLK, BLK).astype(BF16)
        return jnp.dot(vaug[c], p, preferred_element_type=F32)

    peak8 = diagonal(0, s0)
    for i in range(nb):
        src, dst = (s0, s1) if i % 2 == 0 else (s1, s0)
        m = jnp.broadcast_to(jnp.max(peak8, axis=0, keepdims=True), (8, BLK))
        acc[...] = jnp.zeros_like(acc)
        if i + 1 < nb:

            def both(c, peak, i=i, m=m, src=src, dst=dst):
                s = scores(i + 1, c)
                dst[c] = s
                peak = jnp.maximum(peak, fold(s) + (cref[i + 1] - cref[c]))
                acc[...] += weigh(c, m, src, i)
                return peak

            peak8 = lax.fori_loop(0, i + 1, both, jnp.full((8, BLK), -jnp.inf, F32))
            peak8 = jnp.maximum(peak8, diagonal(i + 1, dst))
        else:

            def last(c, _, i=i, m=m, src=src):
                acc[...] += weigh(c, m, src, i)
                return 0

            lax.fori_loop(0, i + 1, last, 0)
        out = (acc[0:64, :] / acc[64:65, :]).astype(BF16)
        for t in range(per):
            o_ref[i * per + t] = out[:, t * TILE : (t + 1) * TILE]


def attend(r):
    n = r.shape[0]
    length = n * TILE
    nb = length // BLK
    vm = pl.BlockSpec(memory_space=pltpu.VMEM)
    return pl.pallas_call(
        attend_kernel,
        out_shape=jax.ShapeDtypeStruct((n, HD, TILE), BF16),
        in_specs=[vm],
        out_specs=vm,
        scratch_shapes=[
            pltpu.VMEM((nb, BLK, 256), BF16),
            pltpu.VMEM((nb, 256, BLK), BF16),
            pltpu.VMEM((nb, 80, BLK), BF16),
            pltpu.VMEM((nb, BLK, BLK), F32),
            pltpu.VMEM((nb, BLK, BLK), F32),
            pltpu.VMEM((80, BLK), F32),
            pltpu.VMEM((nb, 8, BLK), F32),
        ],
        compiler_params=pltpu.CompilerParams(vmem_limit_bytes=40 * 1024 * 1024),
        cost_estimate=pl.CostEstimate(
            flops=2 * length * length * HD, bytes_accessed=3 * 10**6, transcendentals=length * length // 2
        ),
        name="attend",
    )(r)


def local(queries, keys, values, gate_totals, w_out):
    w = lax.all_gather(w_out, "dp", axis=1, tiled=True)
    packed = pack(queries, keys, values, gate_totals)
    held = lax.all_to_all(packed, SP, split_axis=0, concat_axis=0, tiled=True)
    out = attend(held)
    back = lax.all_to_all(out, SP, split_axis=0, concat_axis=0, tiled=True)
    attended = back.reshape(-1, back.shape[2])
    mixed = lax.dot_general(attended, w, (((0,), (0,)), ((), ())), preferred_element_type=F32)
    return mixed.astype(BF16)[None]


def solution(mesh):
    torus = Mesh(mesh.devices.reshape(8, 4, mesh.shape["dp"]), ("sp_0", "sp_1", "dp"))
    rows = P("dp", SP, None)
    return jax.shard_map(
        local, mesh=torus, in_specs=(rows, rows, rows, rows, P(None, "dp")), out_specs=rows, check_vma=False
    )
```

time: 166 us -> 119 us (0.72)
  the two profiles are of different devices: /device:TPU:40 before, /device:TPU:8 now
where the time goes in v1:
time: 119 us; the launch traced here: 118 us
  blocking collectives  77.7 us (65%)
  Pallas kernels  19.6 us (16%)
  between operations  13.4 us (11%)
  matrix products  5.46 us (5%)
  local copies, waits for them, and re-layouts  1.45 us (1%)
    all_to_all x1, blocking collectives, local(): held = lax.all_to_all(packed, SP, split_axis=0, concat_axis=0, tiled=True)  56.1 us
    all_to_all x1, blocking collectives, local(): back = lax.all_to_all(out, SP, split_axis=0, concat_axis=0, tiled=True)  21.6 us
    pallas_call x1, Pallas kernels, attend(): pl.pallas_call(attend_kernel, out_shape=jax.ShapeDtypeStruct((n, HD, TILE...  16.5 us
    dot_general x1, matrix products, local(): lax.dot_general(attended, w, (((0,), (0,)), ((), ())), preferred_element_...  5.46 us
    pallas_call x1, Pallas kernels, pack(): pl.pallas_call(pack_kernel, out_shape=jax.ShapeDtypeStruct((heads, ROWS,...  3.09 us
  transfers between devices with their start and end apart: 1, of which 0 were waited for; matrix products, arithmetic and copies ran while one was open for 1% of the time, Pallas kernels for 17%

profile of v1, /device:TPU:8, one launch (start us, length us, event | category | flops | bytes accessed | tf_op | source)
XLA Modules:
  0.0 118.4 jit_solution(18194944892167745379)
XLA Ops:
  6.5 0.0 all-gather.2.cloned.1.call-start
  6.5 0.7 all-gather.2.cloned.1.call-update
  7.3 1.4 %copy.6.g_ref = f32[1,128,32]{2,1,0:T(8,128)} copy(f32[1,128,32]{1,2,0:T(8,128)} %param.8) | data formatting | bytes 32768 | tf_op args[3]
  8.7 3.1 %pack.1 = bf16[32,208,128]{2,1,0:T(8,128)(2,1)} custom-call(bf16[1,128,2048]{2,1,0:T(8,128)(2,1)} %q_ref.1, bf16[1,128,2048]{2,1,0:T(8,128)(2,1)} %k_ref.1, bf16[1,128,2048]{2,1,0:T(8,128)(2,1)} %v_ref.1, f32[1,128,32]{2,1,0:T(8,128)} %copy.6.g_ref), custom_call_target="tpu_custom_call" | custom-call | flops 10000000 | bytes 4000000 | tf_op jit(solution)/shard_map/pack/pallas_call | solution.py:54
  11.8 56.1 %all_to_all.10.r_ref = bf16[32,208,128]{2,1,0:T(8,128)(2,1)S(1)} all-to-all(bf16[32,208,128]{2,1,0:T(8,128)(2,1)} %pack.1), channel_id=1, replica_groups=mesh['sp_0'=8,'sp_1'=4,'dp'=16] {'sp_0','sp_1'}, dimensions={0} | all-to-all | bytes 3407872 | tf_op jit(solution)/shard_map/all_to_all | solution.py:178
  67.9 16.5 %attend.1 = bf16[32,64,128]{2,1,0:T(8,128)(2,1)S(1)} custom-call(bf16[32,208,128]{2,1,0:T(8,128)(2,1)S(1)} %all_to_all.10.r_ref), custom_call_target="tpu_custom_call" | custom-call | flops 2147483648 | bytes 3000000 | tf_op jit(solution)/shard_map/attend/pallas_call | solution.py:153
  84.4 21.6 %all_to_all.11 = bf16[32,64,128]{2,1,0:T(8,128)(2,1)S(1)} all-to-all(bf16[32,64,128]{2,1,0:T(8,128)(2,1)S(1)} %attend.1), channel_id=1, replica_groups=mesh['sp_0'=8,'sp_1'=4,'dp'=16] {'sp_0','sp_1'}, dimensions={0} | all-to-all | bytes 1048576 | tf_op jit(solution)/shard_map/all_to_all | solution.py:180
  106.1 0.0 all-gather.2.cloned.1.call-done
  106.1 5.5 %fusion = bf16[1,128,2048]{2,1,0:T(8,128)(2,1)} fusion(bf16[2048,128]{1,0:T(8,128)(2,1)S(1)} %bitcast.5, bf16[2048,2048]{1,0:T(8,128)(2,1)} %all-gather.2.cloned.1.call-done), kind=kOutput, calls=%fused_computation.1 | convolution fusion | flops 1074003968 | bytes 9437184 | tf_op jit(solution)/shard_map/dot_general | solution.py:182
Async XLA Ops:
  6.5 99.5 %all-gather.2.cloned.1.call-start = ((), (), s32[]{:S(2)}) async-start(), calls=%async_computation.2 | async-start | bytes 8912896 | tf_op jit(solution)/shard_map/all_gather | solution.py:176
Sparse Core Ops, SparseCore 0:
  9.4 70.7 all-gather.1

commit v2 on v1

v2 whole, which is shorter than its diff:
```python
import math

import jax
import jax.numpy as jnp
from jax import lax
from jax.experimental import pallas as pl
from jax.experimental.pallas import tpu as pltpu
from jax.sharding import Mesh
from jax.sharding import PartitionSpec as P

HD = 64
SP = ("sp_0", "sp_1")
LOG2E = math.log2(math.e)
F32 = jnp.float32
BF16 = jnp.bfloat16
TILE = 128
ROWS = 208
BLK = 512
SUB = 256
PARTS = 4
COLS = 8


def split3(x):
    a = x.astype(BF16)
    r = x - a.astype(F32)
    b = r.astype(BF16)
    c = (r - b.astype(F32)).astype(BF16)
    return a, b, c


def gate_rows(a, b, c):
    row = lax.broadcasted_iota(jnp.int32, (16, a.shape[1]), 0)
    a, b, c = (t.astype(F32) for t in (a, b, c))
    t = jnp.where(row == 0, a, jnp.where(row == 1, b, jnp.where(row == 2, c, 0.0)))
    return t.astype(BF16)


def pack_kernel(q_hbm, k_hbm, v_hbm, g_ref, o_hbm, buf, out, sems, osems):
    heads = out.shape[0]
    part = heads // PARTS
    width = part * HD
    sources = (k_hbm, q_hbm, v_hbm)

    def load(n, s):
        cols = slice(s * width, (s + 1) * width)
        return pltpu.make_async_copy(sources[n].at[0, :, cols], buf.at[n, :, cols], sems.at[n, s])

    def store(s):
        span = slice(s * part, (s + 1) * part)
        return pltpu.make_async_copy(out.at[span], o_hbm.at[span], osems.at[s])

    for s in range(PARTS):
        for n in range(3):
            load(n, s).start()
    a, b, c = (t.astype(F32) for t in split3(g_ref[0]))
    for h in range(heads):
        out[h, 64:80, :] = gate_rows(a[h : h + 1], b[h : h + 1], c[h : h + 1])
    for s in range(PARTS):
        for n, at in enumerate((0, 80, 144)):
            load(n, s).wait()
            for p in range(s * part // 2, (s + 1) * part // 2):
                t = jnp.transpose(buf[n, :, 2 * p * HD : 2 * (p + 1) * HD])
                out[2 * p, at : at + HD, :] = t[:HD]
                out[2 * p + 1, at : at + HD, :] = t[HD:]
        store(s).start()
    for s in range(PARTS):
        store(s).wait()


def pack(q, k, v, g):
    heads = q.shape[2] // HD
    hbm = pl.BlockSpec(memory_space=pl.ANY)
    vm = pl.BlockSpec(memory_space=pltpu.VMEM)
    shape = (heads, ROWS, q.shape[1])
    return pl.pallas_call(
        pack_kernel,
        out_shape=jax.ShapeDtypeStruct(shape, BF16),
        in_specs=[hbm] * 3 + [vm],
        out_specs=hbm,
        scratch_shapes=[
            pltpu.VMEM((3, q.shape[1], q.shape[2]), BF16),
            pltpu.VMEM(shape, BF16),
            pltpu.SemaphoreType.DMA((3, PARTS)),
            pltpu.SemaphoreType.DMA((PARTS,)),
        ],
        cost_estimate=pl.CostEstimate(flops=10**7, bytes_accessed=4 * 10**6, transcendentals=0),
        name="pack",
    )(q, k, v, jnp.swapaxes(g, 1, 2))


def attend_kernel(r_ref, o_ref, kaug, qaug, vaug, s0, s1, acc, cref):
    nb = kaug.shape[0]
    per = BLK // TILE

    rows64 = lax.broadcasted_iota(jnp.int32, (64, BLK), 0)
    ones_rows = jnp.where(rows64 < 3, 1.0, 0.0).astype(BF16)
    vrow = lax.broadcasted_iota(jnp.int32, (16, BLK), 0)
    vones = jnp.where(vrow < 1, 1.0, 0.0).astype(BF16)

    def prepare(c, _):
        gs = []
        for t in range(per):
            g = r_ref[c * per + t, 64:80, :].astype(F32)
            gs.append(g[0:1] + g[1:2] + g[2:3])
        ref = jnp.broadcast_to(gs[-1][:, TILE - 1 : TILE], (1, TILE))
        cref[c] = jnp.broadcast_to(jnp.concatenate([ref] * per, axis=1), (8, BLK))
        for t in range(per):
            j = c * per + t
            lanes = slice(t * TILE, (t + 1) * TILE)
            bias = gate_rows(*split3(ref - gs[t]))
            kt = jnp.concatenate([r_ref[j, 0:64, :], bias, jnp.zeros((48, TILE), BF16)], axis=0)
            kaug[c, lanes, :] = jnp.transpose(kt)
            qaug[c, 0:64, lanes] = r_ref[j, 80:144, :] * BF16(HD**-0.5)
            vaug[c, 0:64, lanes] = r_ref[j, 144:208, :]
        qaug[c, 64:128, :] = ones_rows
        vaug[c, 64:80, :] = vones
        return 0

    lax.fori_loop(0, nb, prepare, 0)

    NS = BLK // SUB

    def fold(s):
        return jnp.max(s.reshape(s.shape[0] // 8, 8, BLK), axis=0)

    def scores(i, c, h):
        return jnp.dot(kaug[c, h * SUB : (h + 1) * SUB, :], qaug[i], preferred_element_type=F32)

    def diagonal(i, dst, h):
        s = scores(i, i, h)
        key = lax.broadcasted_iota(jnp.int32, (SUB, BLK), 0) + h * SUB
        query = lax.broadcasted_iota(jnp.int32, (SUB, BLK), 1)
        s = jnp.where(key <= query, s, -jnp.inf)
        dst[i, h * SUB : (h + 1) * SUB, :] = s
        return fold(s)

    def below(i, c, dst, h):
        s = scores(i, c, h)
        dst[c, h * SUB : (h + 1) * SUB, :] = s
        return fold(s)

    def weigh(c, mm, src, h):
        p = jnp.exp2((src[c, h * SUB : (h + 1) * SUB, :].reshape(SUB // 8, 8, BLK) - mm[None]) * LOG2E)
        p = p.reshape(SUB, BLK).astype(BF16)
        return jnp.dot(vaug[c, :, h * SUB : (h + 1) * SUB], p, preferred_element_type=F32)

    def most(a, b):
        return b if a is None else jnp.maximum(a, b)

    peak8 = None
    for h in range(NS):
        peak8 = most(peak8, diagonal(0, s0, h))
    for i in range(nb):
        src, dst = (s0, s1) if i % 2 == 0 else (s1, s0)
        m = jnp.broadcast_to(jnp.max(peak8, axis=0, keepdims=True), (8, BLK))
        peak8 = None
        total = jnp.zeros(acc.shape, F32)
        for c in range(i + 1):
            mm = m - (cref[i] - cref[c])
            f = None
            for h in range(NS):
                if i + 1 < nb:
                    f = most(f, below(i + 1, c, dst, h))
                total = total + weigh(c, mm, src, h)
            if i + 1 < nb:
                peak8 = most(peak8, f + (cref[i + 1] - cref[c]))
        if i + 1 < nb:
            for h in range(NS):
                peak8 = most(peak8, diagonal(i + 1, dst, h))
        acc[...] = total
        out = (acc[0:64, :] / acc[64:65, :]).astype(BF16)
        for t in range(per):
            o_ref[i * per + t] = out[:, t * TILE : (t + 1) * TILE]


def attend(r):
    n = r.shape[0]
    length = n * TILE
    nb = length // BLK
    vm = pl.BlockSpec(memory_space=pltpu.VMEM)
    return pl.pallas_call(
        attend_kernel,
        out_shape=jax.ShapeDtypeStruct((n, HD, TILE), BF16),
        in_specs=[vm],
        out_specs=vm,
        scratch_shapes=[
            pltpu.VMEM((nb, BLK, 128), BF16),
            pltpu.VMEM((nb, 128, BLK), BF16),
            pltpu.VMEM((nb, 80, BLK), BF16),
            pltpu.VMEM((nb, BLK, BLK), F32),
            pltpu.VMEM((nb, BLK, BLK), F32),
            pltpu.VMEM((80, BLK), F32),
            pltpu.VMEM((nb, 8, BLK), F32),
        ],
        compiler_params=pltpu.CompilerParams(vmem_limit_bytes=40 * 1024 * 1024),
        cost_estimate=pl.CostEstimate(
            flops=2 * length * length * HD, bytes_accessed=3 * 10**6, transcendentals=length * length // 2
        ),
        name="attend",
    )(r)


def project_kernel(a_ref, w_hbm, o_ref, w, sems):
    width = w_hbm.shape[1] // COLS

    def load(s):
        cols = slice(s * width, (s + 1) * width)
        return pltpu.make_async_copy(w_hbm.at[:, cols], w.at[:, cols], sems.at[s])

    for s in range(COLS):
        load(s).start()
    att = jnp.transpose(a_ref[...].reshape(-1, TILE))
    for s in range(COLS):
        load(s).wait()
        cols = slice(s * width, (s + 1) * width)
        o_ref[0, :, cols] = jnp.dot(att, w[:, cols], preferred_element_type=F32).astype(BF16)


def project(attended, w):
    vm = pl.BlockSpec(memory_space=pltpu.VMEM)
    return pl.pallas_call(
        project_kernel,
        out_shape=jax.ShapeDtypeStruct((1, TILE, w.shape[1]), BF16),
        in_specs=[vm, pl.BlockSpec(memory_space=pl.ANY)],
        out_specs=vm,
        scratch_shapes=[pltpu.VMEM(w.shape, BF16), pltpu.SemaphoreType.DMA((COLS,))],
        cost_estimate=pl.CostEstimate(
            flops=2 * TILE * w.size, bytes_accessed=w.size * 2 + 10**6, transcendentals=0
        ),
        name="project",
    )(attended, w)


def local(queries, keys, values, gate_totals, w_out):
    w = lax.all_gather(w_out, "dp", axis=1, tiled=True)
    packed = pack(queries, keys, values, gate_totals)
    held = lax.all_to_all(packed, SP, split_axis=0, concat_axis=0, tiled=True)
    out = attend(held)
    back = lax.all_to_all(out, SP, split_axis=0, concat_axis=0, tiled=True)
    return project(back, w)


def solution(mesh):
    torus = Mesh(mesh.devices.reshape(8, 4, mesh.shape["dp"]), ("sp_0", "sp_1", "dp"))
    rows = P("dp", SP, None)
    return jax.shard_map(
        local, mesh=torus, in_specs=(rows, rows, rows, rows, P(None, "dp")), out_specs=rows, check_vma=False
    )
```

time: 119 us -> 115 us (0.966)
  matrix products: 5.46 us -> 0 us
  Pallas kernels: 19.6 us -> 22.4 us
  local copies, waits for them, and re-layouts: 1.45 us -> 0 us
    pallas_call x1 -> x2, Pallas kernels: 3.09 us -> 10.1 us  [the longest x1 6.5 us: project(): pl.pallas_call(project_kernel, out_shape=jax.ShapeDtypeStruct((1, TILE, w...]
    dot_general x1 -> x0, matrix products: 5.46 us -> none  [local(): lax.dot_general(attended, w, (((0,), (0,)), ((), ())), preferred_element_...]
    pallas_call x1, Pallas kernels: 16.5 us -> 12.3 us  [attend(): pl.pallas_call(attend_kernel, out_shape=jax.ShapeDtypeStruct((n, HD, TILE...]
    unnamed x1 -> x0, local copies, waits for them, and re-layouts: 1.45 us -> none
  transfers between devices with their start and end apart: 1 -> 1, of which waited for: 0 -> 0; matrix products, arithmetic and copies ran while one was open for 1% -> 0% of each run, Pallas kernels for 17% -> 14%
where the time goes in v2:
time: 115 us; the launch traced here: 114 us
  blocking collectives  77.8 us (68%)
  Pallas kernels  22.4 us (19%)
  between operations  13.4 us (12%)
    all_to_all x1, blocking collectives, local(): held = lax.all_to_all(packed, SP, split_axis=0, concat_axis=0, tiled=True)  56.1 us
    all_to_all x1, blocking collectives, local(): back = lax.all_to_all(out, SP, split_axis=0, concat_axis=0, tiled=True)  21.7 us
    pallas_call x1, Pallas kernels, attend(): pl.pallas_call(attend_kernel, out_shape=jax.ShapeDtypeStruct((n, HD, TILE...  12.3 us
    pallas_call x1, Pallas kernels, project(): pl.pallas_call(project_kernel, out_shape=jax.ShapeDtypeStruct((1, TILE, w...  6.5 us
    pallas_call x1, Pallas kernels, pack(): pl.pallas_call(pack_kernel, out_shape=jax.ShapeDtypeStruct(shape, BF16),...  3.62 us
  transfers between devices with their start and end apart: 1, of which 0 were waited for; matrix products, arithmetic and copies ran while one was open for 0% of the time, Pallas kernels for 14%

profile of v2, /device:TPU:8, one launch (start us, length us, event | category | flops | bytes accessed | tf_op | source)
XLA Modules:
  0.0 114.3 jit_solution(9195760044425188125)
XLA Ops:
  6.5 0.0 all-gather.2.cloned.1.call-start
  6.5 0.7 all-gather.2.cloned.1.call-update
  7.3 3.6 %pack.1 = bf16[32,208,128]{2,1,0:T(8,128)(2,1)} custom-call(bf16[1,128,2048]{2,1,0:T(8,128)(2,1)} %q_hbm.1, bf16[1,128,2048]{2,1,0:T(8,128)(2,1)} %k_hbm.1, bf16[1,128,2048]{2,1,0:T(8,128)(2,1)} %v_hbm.1, f32[1,32,128]{2,1,0:T(8,128)} %bitcast.1), custom_call_target="tpu_custom_call" | custom-call | flops 10000000 | bytes 4000000 | tf_op jit(solution)/shard_map/pack/pallas_call | solution.py:76
  10.9 56.1 %all_to_all.10.r_ref = bf16[32,208,128]{2,1,0:T(8,128)(2,1)S(1)} all-to-all(bf16[32,208,128]{2,1,0:T(8,128)(2,1)} %pack.1), channel_id=1, replica_groups=mesh['sp_0'=8,'sp_1'=4,'dp'=16] {'sp_0','sp_1'}, dimensions={0} | all-to-all | bytes 3407872 | tf_op jit(solution)/shard_map/all_to_all | solution.py:238
  67.0 12.3 %attend.1 = bf16[32,64,128]{2,1,0:T(8,128)(2,1)S(1)} custom-call(bf16[32,208,128]{2,1,0:T(8,128)(2,1)S(1)} %all_to_all.10.r_ref), custom_call_target="tpu_custom_call" | custom-call | flops 2147483648 | bytes 3000000 | tf_op jit(solution)/shard_map/attend/pallas_call | solution.py:182
  79.3 21.7 %all_to_all.11.a_ref = bf16[32,64,128]{2,1,0:T(8,128)(2,1)} all-to-all(bf16[32,64,128]{2,1,0:T(8,128)(2,1)S(1)} %attend.1), channel_id=1, replica_groups=mesh['sp_0'=8,'sp_1'=4,'dp'=16] {'sp_0','sp_1'}, dimensions={0} | all-to-all | bytes 1048576 | tf_op jit(solution)/shard_map/all_to_all | solution.py:240
  101.0 0.0 all-gather.2.cloned.1.call-done.w_hbm
  101.0 6.5 %project.1 = bf16[1,128,2048]{2,1,0:T(8,128)(2,1)} custom-call(bf16[32,64,128]{2,1,0:T(8,128)(2,1)} %all_to_all.11.a_ref, bf16[2048,2048]{1,0:T(8,128)(2,1)} %all-gather.2.cloned.1.call-done.w_hbm), custom_call_target="tpu_custom_call" | custom-call | flops 1073741824 | bytes 9388608 | tf_op jit(solution)/shard_map/project/pallas_call | solution.py:222
Async XLA Ops:
  6.5 94.4 %all-gather.2.cloned.1.call-start = ((), (), s32[]{:S(2)}) async-start(), calls=%async_computation.2 | async-start | bytes 8912896 | tf_op jit(solution)/shard_map/all_gather | solution.py:236
Sparse Core Ops, SparseCore 0:
  9.4 70.9 all-gather.1

commit v3 on v2

v3 whole, which is shorter than its diff:
```python
import math

import jax
import jax.numpy as jnp
from jax import lax
from jax.experimental import pallas as pl
from jax.experimental.pallas import tpu as pltpu
from jax.sharding import Mesh
from jax.sharding import PartitionSpec as P

HD = 64
SP = ("sp_0", "sp_1")
LOG2E = math.log2(math.e)
F32 = jnp.float32
BF16 = jnp.bfloat16
TILE = 128
ROWS = 200
BLK = 512
SUB = 256
AHEAD = 6


def split3(x):
    a = x.astype(BF16)
    r = x - a.astype(F32)
    b = r.astype(BF16)
    c = (r - b.astype(F32)).astype(BF16)
    return a, b, c


def gate_rows(a, b, c):
    row = lax.broadcasted_iota(jnp.int32, (8, a.shape[1]), 0)
    a, b, c = (t.astype(F32) for t in (a, b, c))
    t = jnp.where(row == 0, a, jnp.where(row == 1, b, jnp.where(row == 2, c, 0.0)))
    return t.astype(BF16)


def pack_kernel(q_ref, k_ref, v_ref, g_ref, o_ref):
    heads = o_ref.shape[0]
    a, b, c = split3(g_ref[0])
    a, b, c = (t.astype(F32) for t in (a, b, c))
    for p in range(heads // 2):
        cols = slice(2 * p * HD, 2 * (p + 1) * HD)
        for ref, at in ((k_ref, 0), (q_ref, 64), (v_ref, 128)):
            t = jnp.transpose(ref[0, :, cols])
            o_ref[2 * p, at : at + HD, :] = t[:HD]
            o_ref[2 * p + 1, at : at + HD, :] = t[HD:]
    for h in range(heads):
        o_ref[h, 192:200, :] = gate_rows(a[h : h + 1], b[h : h + 1], c[h : h + 1])


def pack(q, k, v, g):
    heads = q.shape[2] // HD
    vm = pl.BlockSpec(memory_space=pltpu.VMEM)
    return pl.pallas_call(
        pack_kernel,
        out_shape=jax.ShapeDtypeStruct((heads, ROWS, q.shape[1]), BF16),
        in_specs=[vm] * 4,
        out_specs=vm,
        cost_estimate=pl.CostEstimate(flops=10**7, bytes_accessed=4 * 10**6, transcendentals=0),
        name="pack",
    )(q, k, v, jnp.swapaxes(g, 1, 2))


def attend_kernel(r_ref, o_ref, kaug, qaug, vaug, s0, s1, acc, cref):
    nb = kaug.shape[0]
    per = BLK // TILE

    rows64 = lax.broadcasted_iota(jnp.int32, (64, BLK), 0)
    ones_rows = jnp.where(rows64 < 3, 1.0, 0.0).astype(BF16)
    vrow = lax.broadcasted_iota(jnp.int32, (16, BLK), 0)
    vones = jnp.where(vrow < 1, 1.0, 0.0).astype(BF16)

    def prepare(c):
        gs = []
        for t in range(per):
            g = r_ref[c * per + t, 192:200, :].astype(F32)
            gs.append(g[0:1] + g[1:2] + g[2:3])
        ref = jnp.broadcast_to(gs[-1][:, TILE - 1 : TILE], (1, TILE))
        cref[c] = jnp.broadcast_to(jnp.concatenate([ref] * per, axis=1), (8, BLK))
        for t in range(per):
            j = c * per + t
            lanes = slice(t * TILE, (t + 1) * TILE)
            bias = gate_rows(*split3(ref - gs[t]))
            kt = jnp.concatenate([r_ref[j, 0:64, :], bias, jnp.zeros((56, TILE), BF16)], axis=0)
            kaug[c, lanes, :] = jnp.transpose(kt)
            qaug[c, 0:64, lanes] = r_ref[j, 64:128, :] * BF16(HD**-0.5)
            vaug[c, 0:64, lanes] = r_ref[j, 128:192, :]
        qaug[c, 64:128, :] = ones_rows
        vaug[c, 64:80, :] = vones

    prepare(0)
    prepare(1)

    NS = BLK // SUB

    def fold(s):
        return jnp.max(s.reshape(s.shape[0] // 8, 8, s.shape[1]), axis=0)

    def scores(i, c, h, at=0):
        return jnp.dot(kaug[c, h * SUB : (h + 1) * SUB, :], qaug[i, :, at:], preferred_element_type=F32)

    def diagonal(i, dst, h):
        at = 0
        s = scores(i, i, h, at)
        key = lax.broadcasted_iota(jnp.int32, s.shape, 0) + h * SUB
        query = lax.broadcasted_iota(jnp.int32, s.shape, 1)
        s = jnp.where(key <= query, s, -jnp.inf)
        dst[i, h * SUB : (h + 1) * SUB, :] = s
        f = fold(s)
        return f if at == 0 else jnp.concatenate([jnp.full((8, at), -jnp.inf, F32), f], axis=1)

    def below(i, c, dst, h):
        s = scores(i, c, h)
        dst[c, h * SUB : (h + 1) * SUB, :] = s
        return fold(s)

    def weigh(total, c, mm, src, h, at=0):
        width = BLK - at
        s = src[c, h * SUB : (h + 1) * SUB, at:].reshape(SUB // 8, 8, width)
        p = jnp.exp2((s - mm[None, :, at:]) * LOG2E).reshape(SUB, width).astype(BF16)
        part = jnp.dot(vaug[c, :, h * SUB : (h + 1) * SUB], p, preferred_element_type=F32)
        if at == 0:
            return total + part
        return jnp.concatenate([total[:, :at], total[:, at:] + part], axis=1)

    def most(a, b):
        return b if a is None else jnp.maximum(a, b)

    peak8 = None
    for h in range(NS):
        peak8 = most(peak8, diagonal(0, s0, h))
    for i in range(nb):
        src, dst = (s0, s1) if i % 2 == 0 else (s1, s0)
        m = jnp.broadcast_to(jnp.max(peak8, axis=0, keepdims=True), (8, BLK))
        peak8 = None
        if i + 2 < nb:
            prepare(i + 2)
        total = jnp.zeros(acc.shape, F32)
        for c in range(i + 1):
            mm = m - (cref[i] - cref[c])
            f = None
            for h in range(NS):
                if i + 1 < nb:
                    f = most(f, below(i + 1, c, dst, h))
                total = weigh(total, c, mm, src, h, 0)
            if i + 1 < nb:
                peak8 = most(peak8, f + (cref[i + 1] - cref[c]))
        if i + 1 < nb:
            for h in range(NS):
                peak8 = most(peak8, diagonal(i + 1, dst, h))
        acc[...] = total
        out = (acc[0:64, :] / acc[64:65, :]).astype(BF16)
        for t in range(per):
            o_ref[i * per + t] = out[:, t * TILE : (t + 1) * TILE]


def attend(r):
    n = r.shape[0]
    length = n * TILE
    nb = length // BLK
    vm = pl.BlockSpec(memory_space=pltpu.VMEM)
    return pl.pallas_call(
        attend_kernel,
        out_shape=jax.ShapeDtypeStruct((n, HD, TILE), BF16),
        in_specs=[vm],
        out_specs=vm,
        scratch_shapes=[
            pltpu.VMEM((nb, BLK, 128), BF16),
            pltpu.VMEM((nb, 128, BLK), BF16),
            pltpu.VMEM((nb, 80, BLK), BF16),
            pltpu.VMEM((nb, BLK, BLK), F32),
            pltpu.VMEM((nb, BLK, BLK), F32),
            pltpu.VMEM((80, BLK), F32),
            pltpu.VMEM((nb, 8, BLK), F32),
        ],
        compiler_params=pltpu.CompilerParams(vmem_limit_bytes=40 * 1024 * 1024),
        cost_estimate=pl.CostEstimate(
            flops=2 * length * length * HD, bytes_accessed=3 * 10**6, transcendentals=length * length // 2
        ),
        name="attend",
    )(r)


def project_kernel(a_hbm, w_hbm, o_hbm, a, w, o, asem, wsems, osems):
    pairs = w_hbm.shape[0] // 2

    def load(s):
        span = pl.ds(2 * s, 2)
        return pltpu.make_async_copy(w_hbm.at[span], w.at[span], wsems.at[s])

    def store(g):
        cols = slice(g * 512, (g + 1) * 512)
        return pltpu.make_async_copy(o.at[:, cols], o_hbm.at[0, :, cols], osems.at[g])

    first = pltpu.make_async_copy(a_hbm, a, asem)
    first.start()
    for s in range(AHEAD):
        load(s).start()
    first.wait()
    att = jnp.transpose(a[...].reshape(-1, TILE))
    for g in range(pairs // 2):
        for s in (2 * g, 2 * g + 1):
            load(s).wait()
            if s + AHEAD < pairs:
                load(s + AHEAD).start()
        quad = jnp.concatenate([w[4 * g + i] for i in range(4)], axis=1)
        o[:, g * 512 : (g + 1) * 512] = jnp.dot(att, quad, preferred_element_type=F32).astype(BF16)
        store(g).start()
    for g in range(pairs // 2):
        store(g).wait()


def project(attended, w):
    hbm = pl.BlockSpec(memory_space=pl.ANY)
    width = w.shape[0] * w.shape[2]
    pairs = w.shape[0] // 2
    return pl.pallas_call(
        project_kernel,
        out_shape=jax.ShapeDtypeStruct((1, TILE, width), BF16),
        in_specs=[hbm, hbm],
        out_specs=hbm,
        scratch_shapes=[
            pltpu.VMEM(attended.shape, BF16),
            pltpu.VMEM(w.shape, BF16),
            pltpu.VMEM((TILE, width), BF16),
            pltpu.SemaphoreType.DMA,
            pltpu.SemaphoreType.DMA((pairs,)),
            pltpu.SemaphoreType.DMA((pairs // 2,)),
        ],
        cost_estimate=pl.CostEstimate(
            flops=2 * TILE * w.size, bytes_accessed=w.size * 2 + 10**6, transcendentals=0
        ),
        name="project",
    )(attended, w)


def local(queries, keys, values, gate_totals, w_out):
    w = lax.all_gather(w_out, "dp", axis=0)
    packed = pack(queries, keys, values, gate_totals)
    held = lax.all_to_all(packed, SP, split_axis=0, concat_axis=0, tiled=True)
    out = attend(held)
    back = lax.all_to_all(out, SP, split_axis=0, concat_axis=0, tiled=True)
    return project(back, w)


def solution(mesh):
    torus = Mesh(mesh.devices.reshape(8, 4, mesh.shape["dp"]), ("sp_0", "sp_1", "dp"))
    rows = P("dp", SP, None)
    return jax.shard_map(
        local, mesh=torus, in_specs=(rows, rows, rows, rows, P(None, "dp")), out_specs=rows, check_vma=False
    )
```

time: 115 us -> 111 us (0.965)
  Pallas kernels: 22.4 us -> 19.9 us
  blocking collectives: 77.8 us -> 76.4 us
    all_to_all x1, blocking collectives: 56.1 us -> 54.8 us  [local(): held = lax.all_to_all(packed, SP, split_axis=0, concat_axis=0, tiled=True)]
  transfers between devices with their start and end apart: 1 -> 1, of which waited for: 0 -> 0; matrix products, arithmetic and copies ran while one was open for 0% -> 0% of each run, Pallas kernels for 14% -> 13%
where the time goes in v3:
time: 111 us; the launch traced here: 110 us
  blocking collectives  76.4 us (69%)
  Pallas kernels  19.9 us (18%)
  between operations  13.4 us (12%)
    all_to_all x1, blocking collectives, local(): held = lax.all_to_all(packed, SP, split_axis=0, concat_axis=0, tiled=True)  54.8 us
    all_to_all x1, blocking collectives, local(): back = lax.all_to_all(out, SP, split_axis=0, concat_axis=0, tiled=True)  21.6 us
    pallas_call x1, Pallas kernels, attend(): pl.pallas_call(attend_kernel, out_shape=jax.ShapeDtypeStruct((n, HD, TILE...  11.2 us
    pallas_call x1, Pallas kernels, project(): pl.pallas_call(project_kernel, out_shape=jax.ShapeDtypeStruct((1, TILE, w...  5.64 us
    pallas_call x1, Pallas kernels, pack(): pl.pallas_call(pack_kernel, out_shape=jax.ShapeDtypeStruct((heads, ROWS,...  3.06 us
  transfers between devices with their start and end apart: 1, of which 0 were waited for; matrix products, arithmetic and copies ran while one was open for 0% of the time, Pallas kernels for 13%

profile of v3, /device:TPU:8, one launch (start us, length us, event | category | flops | bytes accessed | tf_op | source)
XLA Modules:
  0.0 110.4 jit_solution(15283132390651101983)
XLA Ops:
  6.5 0.0 all-gather.3.cloned.1.call-start
  6.5 0.7 all-gather.3.cloned.1.call-update
  7.3 3.1 %pack.1 = bf16[32,200,128]{2,1,0:T(8,128)(2,1)} custom-call(bf16[1,128,2048]{2,1,0:T(8,128)(2,1)} %q_ref.1, bf16[1,128,2048]{2,1,0:T(8,128)(2,1)} %k_ref.1, bf16[1,128,2048]{2,1,0:T(8,128)(2,1)} %v_ref.1, f32[1,32,128]{2,1,0:T(8,128)} %bitcast.3), custom_call_target="tpu_custom_call" | custom-call | flops 10000000 | bytes 4000000 | tf_op jit(solution)/shard_map/pack/pallas_call | solution.py:55
  10.3 54.8 %all_to_all.10.r_ref = bf16[32,200,128]{2,1,0:T(8,128)(2,1)S(1)} all-to-all(bf16[32,200,128]{2,1,0:T(8,128)(2,1)} %pack.1), channel_id=1, replica_groups=mesh['sp_0'=8,'sp_1'=4,'dp'=16] {'sp_0','sp_1'}, dimensions={0} | all-to-all | bytes 3276800 | tf_op jit(solution)/shard_map/all_to_all | solution.py:241
  65.2 11.2 %attend.1 = bf16[32,64,128]{2,1,0:T(8,128)(2,1)S(1)} custom-call(bf16[32,200,128]{2,1,0:T(8,128)(2,1)S(1)} %all_to_all.10.r_ref), custom_call_target="tpu_custom_call" | custom-call | flops 2147483648 | bytes 3000000 | tf_op jit(solution)/shard_map/attend/pallas_call | solution.py:163
  76.3 21.6 %all_to_all.11.a_hbm = bf16[32,64,128]{2,1,0:T(8,128)(2,1)} all-to-all(bf16[32,64,128]{2,1,0:T(8,128)(2,1)S(1)} %attend.1), channel_id=1, replica_groups=mesh['sp_0'=8,'sp_1'=4,'dp'=16] {'sp_0','sp_1'}, dimensions={0} | all-to-all | bytes 1048576 | tf_op jit(solution)/shard_map/all_to_all | solution.py:243
  97.9 0.0 all-gather.3.cloned.1.call-done
  97.9 5.6 %project.1 = bf16[1,128,2048]{2,1,0:T(8,128)(2,1)} custom-call(bf16[32,64,128]{2,1,0:T(8,128)(2,1)} %all_to_all.11.a_hbm, bf16[16,2048,128]{2,1,0:T(8,128)(2,1)} %bitcast.2), custom_call_target="tpu_custom_call" | custom-call | flops 1073741824 | bytes 9388608 | tf_op jit(solution)/shard_map/project/pallas_call | solution.py:218
Async XLA Ops:
  6.5 91.4 %all-gather.3.cloned.1.call-start = ((), (), s32[]{:S(2)}) async-start(), calls=%async_computation.2 | async-start | bytes 8912896 | tf_op jit(solution)/shard_map/all_gather | solution.py:239
Sparse Core Ops, SparseCore 0:
  9.4 61.2 all-gather.2

commit v4 on v3

--- a/solution.py
+++ b/solution.py
@@ -35,28 +35,53 @@
     return t.astype(BF16)
 
 
-def pack_kernel(q_ref, k_ref, v_ref, g_ref, o_ref):
-    heads = o_ref.shape[0]
-    a, b, c = split3(g_ref[0])
-    a, b, c = (t.astype(F32) for t in (a, b, c))
-    for p in range(heads // 2):
-        cols = slice(2 * p * HD, 2 * (p + 1) * HD)
-        for ref, at in ((k_ref, 0), (q_ref, 64), (v_ref, 128)):
-            t = jnp.transpose(ref[0, :, cols])
-            o_ref[2 * p, at : at + HD, :] = t[:HD]
-            o_ref[2 * p + 1, at : at + HD, :] = t[HD:]
+def pack_kernel(q_hbm, k_hbm, v_hbm, g_hbm, o_hbm, buf, g, out, sems, osems):
+    heads = out.shape[0]
+    sources = (k_hbm, q_hbm, v_hbm)
+
+    def load(n):
+        return pltpu.make_async_copy(sources[n].at[0], buf.at[n], sems.at[n])
+
+    def store(n):
+        rows = slice(n * HD, (n + 1) * HD if n < 3 else ROWS)
+        return pltpu.make_async_copy(out.at[:, rows, :], o_hbm.at[:, rows, :], osems.at[n])
+
+    gates = pltpu.make_async_copy(g_hbm.at[0], g, sems.at[3])
+    gates.start()
+    for n in range(3):
+        load(n).start()
+    gates.wait()
+    a, b, c = (t.astype(F32) for t in split3(g[...]))
     for h in range(heads):
-        o_ref[h, 192:200, :] = gate_rows(a[h : h + 1], b[h : h + 1], c[h : h + 1])
+        out[h, 192:200, :] = gate_rows(a[h : h + 1], b[h : h + 1], c[h : h + 1])
+    store(3).start()
+    for n in range(3):
+        load(n).wait()
+        for p in range(heads // 2):
+            t = jnp.transpose(buf[n, :, 2 * p * HD : 2 * (p + 1) * HD])
+            out[2 * p, n * HD : (n + 1) * HD, :] = t[:HD]
+            out[2 * p + 1, n * HD : (n + 1) * HD, :] = t[HD:]
+        store(n).start()
+    for n in range(4):
+        store(n).wait()
 
 
 def pack(q, k, v, g):
     heads = q.shape[2] // HD
-    vm = pl.BlockSpec(memory_space=pltpu.VMEM)
+    hbm = pl.BlockSpec(memory_space=pl.ANY)
+    shape = (heads, ROWS, q.shape[1])
     return pl.pallas_call(
         pack_kernel,
-        out_shape=jax.ShapeDtypeStruct((heads, ROWS, q.shape[1]), BF16),
-        in_specs=[vm] * 4,
-        out_specs=vm,
+        out_shape=jax.ShapeDtypeStruct(shape, BF16),
+        in_specs=[hbm] * 4,
+        out_specs=hbm,
+        scratch_shapes=[
+            pltpu.VMEM((3, q.shape[1], q.shape[2]), BF16),
+            pltpu.VMEM((heads, q.shape[1]), F32),
+            pltpu.VMEM(shape, BF16),
+            pltpu.SemaphoreType.DMA((4,)),
+            pltpu.SemaphoreType.DMA((4,)),
+        ],
         cost_estimate=pl.CostEstimate(flops=10**7, bytes_accessed=4 * 10**6, transcendentals=0),
         name="pack",
     )(q, k, v, jnp.swapaxes(g, 1, 2))

time: 111 us -> 110 us (level)
  the two profiles are of different devices: /device:TPU:8 before, /device:TPU:16 now
where the time goes in v4:
time: 110 us
  blocking collectives  76.5 us (70%)
  Pallas kernels  19.4 us (18%)
  between operations  13.4 us (12%)
    all_to_all x1, blocking collectives, local(): held = lax.all_to_all(packed, SP, split_axis=0, concat_axis=0, tiled=True)  54.9 us
    all_to_all x1, blocking collectives, local(): back = lax.all_to_all(out, SP, split_axis=0, concat_axis=0, tiled=True)  21.6 us
    pallas_call x1, Pallas kernels, attend(): pl.pallas_call(attend_kernel, out_shape=jax.ShapeDtypeStruct((n, HD, TILE...  11.2 us
    pallas_call x1, Pallas kernels, project(): pl.pallas_call(project_kernel, out_shape=jax.ShapeDtypeStruct((1, TILE, w...  5.64 us
    pallas_call x1, Pallas kernels, pack(): pl.pallas_call(pack_kernel, out_shape=jax.ShapeDtypeStruct(shape, BF16),...  2.6 us
  transfers between devices with their start and end apart: 1, of which 0 were waited for; matrix products, arithmetic and copies ran while one was open for 0% of the time, Pallas kernels for 13%

profile of v4, /device:TPU:16, one launch (start us, length us, event | category | flops | bytes accessed | tf_op | source)
XLA Modules:
  0.0 110.0 jit_solution(10885352138484472757)
XLA Ops:
  6.5 0.0 all-gather.3.cloned.1.call-start
  6.5 0.7 all-gather.3.cloned.1.call-update
  7.3 2.6 %pack.1 = bf16[32,200,128]{2,1,0:T(8,128)(2,1)} custom-call(bf16[1,128,2048]{2,1,0:T(8,128)(2,1)} %q_hbm.1, bf16[1,128,2048]{2,1,0:T(8,128)(2,1)} %k_hbm.1, bf16[1,128,2048]{2,1,0:T(8,128)(2,1)} %v_hbm.1, f32[1,32,128]{2,1,0:T(8,128)} %bitcast.3), custom_call_target="tpu_custom_call" | custom-call | flops 10000000 | bytes 4000000 | tf_op jit(solution)/shard_map/pack/pallas_call | solution.py:73
  9.9 54.9 %all_to_all.10.r_ref = bf16[32,200,128]{2,1,0:T(8,128)(2,1)S(1)} all-to-all(bf16[32,200,128]{2,1,0:T(8,128)(2,1)} %pack.1), channel_id=1, replica_groups=mesh['sp_0'=8,'sp_1'=4,'dp'=16] {'sp_0','sp_1'}, dimensions={0} | all-to-all | bytes 3276800 | tf_op jit(solution)/shard_map/all_to_all | solution.py:266
  64.7 11.2 %attend.1 = bf16[32,64,128]{2,1,0:T(8,128)(2,1)S(1)} custom-call(bf16[32,200,128]{2,1,0:T(8,128)(2,1)S(1)} %all_to_all.10.r_ref), custom_call_target="tpu_custom_call" | custom-call | flops 2147483648 | bytes 3000000 | tf_op jit(solution)/shard_map/attend/pallas_call | solution.py:188
  75.9 21.6 %all_to_all.11.a_hbm = bf16[32,64,128]{2,1,0:T(8,128)(2,1)} all-to-all(bf16[32,64,128]{2,1,0:T(8,128)(2,1)S(1)} %attend.1), channel_id=1, replica_groups=mesh['sp_0'=8,'sp_1'=4,'dp'=16] {'sp_0','sp_1'}, dimensions={0} | all-to-all | bytes 1048576 | tf_op jit(solution)/shard_map/all_to_all | solution.py:268
  97.5 0.0 all-gather.3.cloned.1.call-done
  97.5 5.6 %project.1 = bf16[1,128,2048]{2,1,0:T(8,128)(2,1)} custom-call(bf16[32,64,128]{2,1,0:T(8,128)(2,1)} %all_to_all.11.a_hbm, bf16[16,2048,128]{2,1,0:T(8,128)(2,1)} %bitcast.2), custom_call_target="tpu_custom_call" | custom-call | flops 1073741824 | bytes 9388608 | tf_op jit(solution)/shard_map/project/pallas_call | solution.py:243
Async XLA Ops:
  6.5 91.0 %all-gather.3.cloned.1.call-start = ((), (), s32[]{:S(2)}) async-start(), calls=%async_computation.2 | async-start | bytes 8912896 | tf_op jit(solution)/shard_map/all_gather | solution.py:264
Sparse Core Ops, SparseCore 0:
  9.4 61.1 all-gather.2
